TPU v7x, 32 devices: a whole 2x2x4 slice. The times are simulated.
32 devices in a mesh: sp: 8 (over z, x), tp: 4 (over y, core).
Axes of the slice: x: 2, y: 2, z: 4, core: 2. Of those that a mesh axis runs over, the one named last changes fastest.
Arguments:
- tokens: bfloat16 [2, 1536, 4096], P(None, 'sp', 'tp'), may hold values from -12 to 12
- query_weight: bfloat16 [4096, 2048], P(None, 'tp'), may hold values from -0.09375 to 0.09375
- key_weight: bfloat16 [4096, 2048], P(None, 'tp'), may hold values from -0.09375 to 0.09375
- value_weight: bfloat16 [4096, 2048], P(None, 'tp'), may hold values from -0.09375 to 0.09375
- gate_weight: bfloat16 [4096, 2048], P(None, 'tp'), may hold values from -0.09375 to 0.09375
- beta_weight: bfloat16 [4096, 16], P(None, 'tp'), may hold values from -0.09375 to 0.09375
- decay_weight: bfloat16 [4096, 16], P(None, 'tp'), may hold values from -0.09375 to 0.09375
- beta_bias: float32 [16], P('tp'), may hold values from -6 to -3
- rate_log: float32 [16], P('tp'), may hold values from -12 to -2.5
- out_gain: float32 [128], replicated, may hold values from 0.1 to 1.9
- new_query: bfloat16 [2, 16, 128], P(None, 'tp'), may hold values from -6 to 6
- new_key: bfloat16 [2, 16, 128], P(None, 'tp'), may hold values from -6 to 6
- new_value: bfloat16 [2, 16, 128], P(None, 'tp'), may hold values from -6 to 6
- new_beta: float32 [2, 16], P(None, 'tp'), may hold values from 0.1 to 0.9
- new_decay: float32 [2, 16], P(None, 'tp'), may hold values from 0.3 to 1
Outputs:
- mixed_out: bfloat16 [2, 1536, 2048], P(None, 'sp', 'tp')
- cache: bfloat16 [2, 16, 128, 128], P(None, 'tp', 'sp')
- first_out: float32 [2, 2048], P(None, 'tp')
All inputs are finite; a program needn't handle non-finite values.
Results may differ from a plain program's by a relative error of at most 0.0073.
Values may be sent and summed in bfloat16 or wider, within the bound.
A program may use at most 64 MiB of HBM per device.

v0:
```python
import jax
import jax.numpy as jnp
from jax import lax
from jax.sharding import PartitionSpec as P

BLOCK = 64
unit_floor = 1.0
norm_floor = 0.001
highest = lax.Precision.HIGHEST


def shifted(value, axis, steps):
    count = lax.axis_size(axis)
    first, last = (max(0, -steps), min(count, count - steps))
    return lax.ppermute(value, axis, [(source, source + steps) for source in range(first, last)])


def matmul(form, left, right):
    return jnp.einsum(form, left, right, precision=highest)


def unit_rows(values):
    return values * lax.rsqrt(jnp.sum(values * values, axis=-1, keepdims=True) + unit_floor)


def head_norm(values, out_gain):
    return (
        values
        * lax.rsqrt(jnp.mean(values * values, axis=-1, keepdims=True) + norm_floor)
        * out_gain
    )


def stored(values):
    return lax.optimization_barrier(values.astype(jnp.bfloat16)).astype(jnp.float32)


def unit_lower_inverse(lower_part):
    extent = lower_part.shape[-1]
    nilpotent = -lower_part
    inverse = jnp.eye(extent, dtype=jnp.float32) + nilpotent
    for _ in range(extent.bit_length() - 2):
        nilpotent = matmul("...ij,...jk->...ik", nilpotent, nilpotent)
        inverse = inverse + matmul("...ij,...jk->...ik", nilpotent, inverse)
    return inverse


def prepare(
    query_rows,
    key_rows,
    value_rows,
    beta_in,
    decay_in,
    beta_bias,
    rate_log,
    seq_count,
    length,
    head_count,
):
    extent = query_rows.shape[-1] // head_count
    blocks = length // BLOCK

    def by_head(values):
        shaped = values.reshape(seq_count, blocks, BLOCK, head_count, extent)
        return shaped.transpose(0, 3, 1, 2, 4).reshape(
            seq_count * head_count, blocks, BLOCK, extent
        )

    def by_scalar(values):
        shaped = values.reshape(seq_count, blocks, BLOCK, head_count)
        return shaped.transpose(0, 3, 1, 2).reshape(seq_count * head_count, blocks, BLOCK)

    queries = unit_rows(by_head(query_rows))
    key_unit = unit_rows(by_head(key_rows))
    values = by_head(value_rows)
    strength = by_scalar(jax.nn.sigmoid(beta_in + beta_bias))
    decays = by_scalar(-jnp.exp(rate_log) * jax.nn.softplus(decay_in))
    return (queries, key_unit, values, strength, decays)


def block_terms(queries, key_unit, values, strength, decays):
    extent = decays.shape[-1]
    cumulative = jnp.cumsum(decays, axis=-1)
    causal = jnp.tril(jnp.ones((extent, extent), bool))
    strict = jnp.tril(jnp.ones((extent, extent), bool), -1)
    spread = cumulative[..., :, None] - cumulative[..., None, :]
    weights = jnp.where(causal, jnp.exp(jnp.where(causal, spread, 0.0)), 0.0)
    key_beta = key_unit * strength[..., None]
    lower_part = jnp.where(strict, matmul("...td,...sd->...ts", key_beta, key_unit) * weights, 0.0)
    inverse = unit_lower_inverse(lower_part)
    update = matmul("...ts,...se->...te", inverse, values * strength[..., None])
    carry_w = matmul("...ts,...sd->...td", inverse, key_beta * jnp.exp(cumulative)[..., None])
    scores = matmul("...td,...sd->...ts", queries, key_unit) * weights
    query_decay = queries * jnp.exp(cumulative)[..., None]
    last_log = cumulative[..., -1]
    key_decay = key_unit * jnp.exp(last_log[..., None] - cumulative)[..., None]
    return (update, carry_w, query_decay, scores, key_decay, last_log)


def finish_read(recall, retrieve, query_unit, key_unit, new_value, new_beta, new_decay, out_gain):
    seq_count, head_count, extent = recall.shape
    intersect = jnp.sum(key_unit * query_unit, axis=-1)
    fresh_values = new_value.astype(jnp.float32) - new_decay[..., None] * retrieve
    read_heads = new_decay[..., None] * recall + (new_beta * intersect)[..., None] * fresh_values
    return head_norm(read_heads, out_gain).reshape(seq_count, head_count * extent)


def project_rows(shard_rows, weights):
    row_count = shard_rows.shape[-1]
    flat_rows = shard_rows.reshape(-1, row_count)
    return tuple(
        (jnp.dot(flat_rows, weight, preferred_element_type=jnp.float32) for weight in weights)
    )


def shards(
    tokens,
    query_weight,
    key_weight,
    value_weight,
    gate_weight,
    beta_weight,
    decay_weight,
    beta_bias,
    rate_log,
    out_gain,
    new_query,
    new_key,
    new_value,
    new_beta,
    new_decay,
):
    seq_count, span_len, _ = tokens.shape
    head_count = rate_log.shape[0]
    weights = (query_weight, key_weight, value_weight, gate_weight, beta_weight, decay_weight)
    totals = project_rows(lax.all_gather(tokens, "tp", axis=2, tiled=True), weights)
    query_rows = stored(totals[0])
    key_rows = stored(totals[1])
    value_rows = stored(totals[2])
    gate_rows = stored(totals[3])
    prepared = prepare(
        query_rows,
        key_rows,
        value_rows,
        totals[4],
        totals[5],
        beta_bias,
        rate_log,
        seq_count,
        span_len,
        head_count,
    )
    block_data = block_terms(*prepared)
    batch_size = block_data[0].shape[0]
    extent = block_data[0].shape[-1]
    identity = jnp.broadcast_to(jnp.eye(extent, dtype=jnp.float32), (batch_size, extent, extent))

    def advance(carried, inputs):
        state_now, reach_map = carried
        u_block, w_block, qg_block, score_block, kd_block, gl_block = inputs
        fresh_values = u_block - matmul("btd,bde->bte", w_block, state_now)
        block_out = matmul("btd,bde->bte", qg_block, state_now) + matmul(
            "bts,bse->bte", score_block, fresh_values
        )
        reach_rows = qg_block - matmul("bts,bsd->btd", score_block, w_block)
        factor = jnp.exp(gl_block)[:, None, None]
        transit = factor * identity - matmul("bsd,bse->bde", kd_block, w_block)
        state_next = state_now * factor + matmul("bsd,bse->bde", kd_block, fresh_values)
        map_next = matmul("bde,bef->bdf", transit, reach_map)
        return ((state_next, map_next), (block_out, matmul("btd,bde->bte", reach_rows, reach_map)))

    inputs = tuple((jnp.moveaxis(member, 1, 0) for member in block_data))
    start_state = jnp.zeros((batch_size, extent, extent), jnp.float32)
    (local_state, local_map), (local_out, reach_all) = lax.scan(
        advance, (start_state, identity), inputs
    )

    def turn(turn_index, incoming):
        outgoing = matmul("bde,bef->bdf", local_map, incoming) + local_state
        return shifted(outgoing, "sp", 1)

    incoming = lax.fori_loop(0, lax.axis_size("sp") - 1, turn, jnp.zeros_like(local_state))
    block_total = local_out + matmul("nbtd,bde->nbte", reach_all, incoming)
    blocks = span_len // BLOCK
    heads_out = block_total.reshape(blocks, seq_count, head_count, BLOCK, extent).transpose(
        1, 0, 3, 2, 4
    )
    heads_out = heads_out.reshape(seq_count, span_len, head_count, extent)
    gate_values = gate_rows.reshape(seq_count, span_len, head_count, extent)
    mixed_out = (head_norm(heads_out, out_gain) * jax.nn.silu(gate_values)).astype(jnp.bfloat16)
    mixed_out = mixed_out.reshape(seq_count, span_len, head_count * extent)
    final_state = matmul("bde,bef->bdf", local_map, incoming) + local_state
    final_cast = final_state.reshape(seq_count, head_count, extent, extent).astype(jnp.bfloat16)
    row_count = extent // lax.axis_size("sp")
    row_start = lax.axis_index("sp") * row_count
    query_unit = unit_rows(new_query.astype(jnp.float32))
    key_unit = unit_rows(new_key.astype(jnp.float32))
    is_last = lax.axis_index("sp") == lax.axis_size("sp") - 1
    own_term = jnp.where(is_last, final_cast.astype(jnp.float32), 0.0)
    cache_rows = lax.psum_scatter(
        own_term.astype(jnp.bfloat16), "sp", scatter_dimension=2, tiled=True
    )
    memory = lax.optimization_barrier(cache_rows).astype(jnp.float32)
    query_part = lax.dynamic_slice_in_dim(query_unit, row_start, row_count, 2)
    key_part = lax.dynamic_slice_in_dim(key_unit, row_start, row_count, 2)
    recall, retrieve = lax.psum(
        (matmul("shde,shd->she", memory, query_part), matmul("shde,shd->she", memory, key_part)),
        "sp",
    )
    first_out = finish_read(
        recall, retrieve, query_unit, key_unit, new_value, new_beta, new_decay, out_gain
    )
    return (mixed_out, cache_rows, first_out)


def solution(mesh):
    placed = (
        P(None, "sp", "tp"),
        P(None, "tp"),
        P(None, "tp"),
        P(None, "tp"),
        P(None, "tp"),
        P(None, "tp"),
        P(None, "tp"),
        P("tp"),
        P("tp"),
        P(),
        P(None, "tp", None),
        P(None, "tp", None),
        P(None, "tp", None),
        P(None, "tp"),
        P(None, "tp"),
    )
    return jax.shard_map(
        shards,
        mesh=mesh,
        in_specs=placed,
        out_specs=(P(None, "sp", "tp"), P(None, "tp", "sp", None), P(None, "tp")),
        check_vma=False,
    )
```

profile of v0, /device:TPU:0, one launch (start us, length us, event | category | flops | bytes accessed | tf_op | source)
XLA Modules:
  0.0 305.5 jit_solution(13586617555090404799)
XLA Ops:
  7.2 0.7 all-gather.2.cloned.1.call-update
  8.0 0.8 fusion.67
  8.8 0.8 fusion.68
  9.5 0.9 multiply_reduce_fusion.4
  13.8 27.1 %all-gather.2.cloned.1.call-done = bf16[2,192,4096]{2,1,0:T(8,128)(2,1)} async-done(((bf16[2,192,1024]{2,1,0:T(8,128)(2,1)}), bf16[2,192,4096]{2,1,0:T(8,128)(2,1)}) %all-gather.2.cloned.1.call-update) | async-done | bytes 3145744 | tf_op jit(solution)/shard_map/all_gather | solution.py:136
  40.9 2.8 fusion.66
  44.7 5.8 %convolution_convert_fusion = bf16[384,512]{1,0:T(8,128)(2,1)} fusion(bf16[384,4096]{1,0:T(8,128)(2,1)} %bitcast.200, bf16[4096,512]{1,0:T(8,128)(2,1)} %param.23), kind=kOutput, calls=%fused_computation.59 | convolution fusion | flops 1610809344 | bytes 7733248 | tf_op jit(solution)/shard_map/dot_general | solution.py:112
  50.6 1.8 convolution_convert_fusion.1
  53.4 2.8 fusion.49
  56.3 4.9 %convolution_convert_fusion.3 = bf16[384,512]{1,0:T(8,128)(2,1)S(1)} fusion(bf16[384,4096]{1,0:T(8,128)(2,1)} %bitcast.202, bf16[4096,512]{1,0:T(8,128)(2,1)} %param.21), kind=kOutput, calls=%fused_computation.62 | convolution fusion | flops 1610809344 | bytes 7733248 | tf_op jit(solution)/shard_map/dot_general | solution.py:112
  62.2 4.9 %convolution_convert_fusion.2 = bf16[384,512]{1,0:T(8,128)(2,1)S(1)} fusion(bf16[384,4096]{1,0:T(8,128)(2,1)} %bitcast.203, bf16[4096,512]{1,0:T(8,128)(2,1)} %param.22), kind=kOutput, calls=%fused_computation.61 | convolution fusion | flops 1610809344 | bytes 7733248 | tf_op jit(solution)/shard_map/dot_general | solution.py:112
  67.6 1.2 multiply_bitcast_fusion
  69.0 1.4 fusion.41
  70.5 0.9 fusion.70
  71.4 0.9 fusion.71
  72.3 0.9 convolution_add_fusion.7
  73.2 0.9 fusion.72
  74.2 0.9 convolution_add_fusion.6
  75.1 0.9 fusion.73
  76.0 0.9 convolution_add_fusion.5
  76.9 0.9 fusion.74
  77.8 0.9 convolution_add_fusion.4
  78.7 0.9 convolution_add_fusion.3
  79.7 2.0 convolution_bitcast_fusion.4
  81.7 0.9 convolution_bitcast_fusion.3
  82.6 2.3 fusion.38
  85.0 23.5 %while.28 = (s32[]{:T(128)}, f32[8,128,128]{2,1,0:T(8,128)S(1)}, f32[8,128,128]{2,1,0:T(8,128)S(1)}, f32[3,8,64,128]{3,2,0,1:T(8,128)}, f32[3,8,64,128]{3,2,0,1:...) while((s32[]{:T(128)}, f32[8,128,128]{2,1,0:T(8,128)S(1)}, ...), condition=%wide.region_4.5_spmd.clone, body=%wide.region_3.4_spmd.clone.sunk | while | flops 806420480 | bytes 12392708 | solution.py:174
  85.6 1.5 convolution_subtract_fusion.6
  87.2 1.1 convolution_add_fusion.13
  88.7 1.3 fusion.170
  90.0 1.0 convolution_subtract_fusion.7
  91.7 1.1 fusion.169
  93.4 1.5 convolution_subtract_fusion.6
  95.0 1.1 convolution_add_fusion.13
  96.6 1.3 fusion.170
  97.9 1.0 convolution_subtract_fusion.7
  99.6 1.1 fusion.169
  101.3 1.5 convolution_subtract_fusion.6
  102.8 1.1 convolution_add_fusion.13
  104.4 1.3 fusion.170
  105.7 1.0 convolution_subtract_fusion.7
  107.4 1.1 fusion.169
  108.5 101.1 %while.27 = (s32[]{:T(128)}, f32[8,128,128]{2,1,0:T(8,128)S(1)}, f32[8,128,128]{2,1,0:T(8,128)S(1)}, f32[8,128,128]{2,1,0:T(8,128)S(1)}, s32[]{:T(128)}) while((s32[]{:T(128)}, f32[8,128,128]{2,1,0:T(8,128)S(1)}, f32[8,128,128]{2,1,0:T(8,128)S(1)}, f32[8,128,128]{2,1,0:T(8,128)S(1)}, s32[]{:T(128)}) %tuple.60), condition=%wide.region_6.7_spmd, body=%wide.region_5.6_spmd.sunk | while | flops 201457664 | bytes 4194405 | solution.py:182
  109.2 3.4 %collective-permute-start = (f32[8,128,128]{2,1,0:T(8,128)S(1)}, f32[8,128,128]{2,1,0:T(8,128)S(1)}, u32[]{:S(2)}, u32[]{:S(2)}) collective-permute-start(f32[8,128,128]{2,1,0:T(8,128)S(1)} %convolution_add_fusion.12), channel_id=1, source_target_pairs={{0,4},{4,8},{8,12},{12,16},{16,20},{20,24},{24,28},{1,5},{5,9},{9,... | collective-permute-start | bytes 1572872 | tf_op jit(solution)/shard_map/while/body/eval_jaxpr/ppermute | solution.py:15
  112.6 11.5 %collective-permute-done = f32[8,128,128]{2,1,0:T(8,128)S(1)} collective-permute-done((f32[8,128,128]{2,1,0:T(8,128)S(1)}, f32[8,128,128]{2,1,0:T(8,128)S(1)}, u32[]{:S(2)}, u32[]{:S(2)}) %collective-permute-start) | collective-permute-done | bytes 524320 | tf_op jit(solution)/shard_map/while/body/eval_jaxpr/ppermute | solution.py:15
  124.8 4.4 %collective-permute-start = (f32[8,128,128]{2,1,0:T(8,128)S(1)}, f32[8,128,128]{2,1,0:T(8,128)S(1)}, u32[]{:S(2)}, u32[]{:S(2)}) collective-permute-start(f32[8,128,128]{2,1,0:T(8,128)S(1)} %convolution_add_fusion.12), channel_id=1, source_target_pairs={{0,4},{4,8},{8,12},{12,16},{16,20},{20,24},{24,28},{1,5},{5,9},{9,... | collective-permute-start | bytes 1572872 | tf_op jit(solution)/shard_map/while/body/eval_jaxpr/ppermute | solution.py:15
  129.2 10.7 %collective-permute-done = f32[8,128,128]{2,1,0:T(8,128)S(1)} collective-permute-done((f32[8,128,128]{2,1,0:T(8,128)S(1)}, f32[8,128,128]{2,1,0:T(8,128)S(1)}, u32[]{:S(2)}, u32[]{:S(2)}) %collective-permute-start) | collective-permute-done | bytes 524320 | tf_op jit(solution)/shard_map/while/body/eval_jaxpr/ppermute | solution.py:15
  140.6 4.4 %collective-permute-start = (f32[8,128,128]{2,1,0:T(8,128)S(1)}, f32[8,128,128]{2,1,0:T(8,128)S(1)}, u32[]{:S(2)}, u32[]{:S(2)}) collective-permute-start(f32[8,128,128]{2,1,0:T(8,128)S(1)} %convolution_add_fusion.12), channel_id=1, source_target_pairs={{0,4},{4,8},{8,12},{12,16},{16,20},{20,24},{24,28},{1,5},{5,9},{9,... | collective-permute-start | bytes 1572872 | tf_op jit(solution)/shard_map/while/body/eval_jaxpr/ppermute | solution.py:15
  145.0 9.8 %collective-permute-done = f32[8,128,128]{2,1,0:T(8,128)S(1)} collective-permute-done((f32[8,128,128]{2,1,0:T(8,128)S(1)}, f32[8,128,128]{2,1,0:T(8,128)S(1)}, u32[]{:S(2)}, u32[]{:S(2)}) %collective-permute-start) | collective-permute-done | bytes 524320 | tf_op jit(solution)/shard_map/while/body/eval_jaxpr/ppermute | solution.py:15
  155.5 5.2 %collective-permute-start = (f32[8,128,128]{2,1,0:T(8,128)S(1)}, f32[8,128,128]{2,1,0:T(8,128)S(1)}, u32[]{:S(2)}, u32[]{:S(2)}) collective-permute-start(f32[8,128,128]{2,1,0:T(8,128)S(1)} %convolution_add_fusion.12), channel_id=1, source_target_pairs={{0,4},{4,8},{8,12},{12,16},{16,20},{20,24},{24,28},{1,5},{5,9},{9,... | collective-permute-start | bytes 1572872 | tf_op jit(solution)/shard_map/while/body/eval_jaxpr/ppermute | solution.py:15
  160.7 9.0 %collective-permute-done = f32[8,128,128]{2,1,0:T(8,128)S(1)} collective-permute-done((f32[8,128,128]{2,1,0:T(8,128)S(1)}, f32[8,128,128]{2,1,0:T(8,128)S(1)}, u32[]{:S(2)}, u32[]{:S(2)}) %collective-permute-start) | collective-permute-done | bytes 524320 | tf_op jit(solution)/shard_map/while/body/eval_jaxpr/ppermute | solution.py:15
  170.3 5.3 %collective-permute-start = (f32[8,128,128]{2,1,0:T(8,128)S(1)}, f32[8,128,128]{2,1,0:T(8,128)S(1)}, u32[]{:S(2)}, u32[]{:S(2)}) collective-permute-start(f32[8,128,128]{2,1,0:T(8,128)S(1)} %convolution_add_fusion.12), channel_id=1, source_target_pairs={{0,4},{4,8},{8,12},{12,16},{16,20},{20,24},{24,28},{1,5},{5,9},{9,... | collective-permute-start | bytes 1572872 | tf_op jit(solution)/shard_map/while/body/eval_jaxpr/ppermute | solution.py:15
  175.7 8.1 %collective-permute-done = f32[8,128,128]{2,1,0:T(8,128)S(1)} collective-permute-done((f32[8,128,128]{2,1,0:T(8,128)S(1)}, f32[8,128,128]{2,1,0:T(8,128)S(1)}, u32[]{:S(2)}, u32[]{:S(2)}) %collective-permute-start) | collective-permute-done | bytes 524320 | tf_op jit(solution)/shard_map/while/body/eval_jaxpr/ppermute | solution.py:15
  184.4 5.3 %collective-permute-start = (f32[8,128,128]{2,1,0:T(8,128)S(1)}, f32[8,128,128]{2,1,0:T(8,128)S(1)}, u32[]{:S(2)}, u32[]{:S(2)}) collective-permute-start(f32[8,128,128]{2,1,0:T(8,128)S(1)} %convolution_add_fusion.12), channel_id=1, source_target_pairs={{0,4},{4,8},{8,12},{12,16},{16,20},{20,24},{24,28},{1,5},{5,9},{9,... | collective-permute-start | bytes 1572872 | tf_op jit(solution)/shard_map/while/body/eval_jaxpr/ppermute | solution.py:15
  189.8 7.3 %collective-permute-done = f32[8,128,128]{2,1,0:T(8,128)S(1)} collective-permute-done((f32[8,128,128]{2,1,0:T(8,128)S(1)}, f32[8,128,128]{2,1,0:T(8,128)S(1)}, u32[]{:S(2)}, u32[]{:S(2)}) %collective-permute-start) | collective-permute-done | bytes 524320 | tf_op jit(solution)/shard_map/while/body/eval_jaxpr/ppermute | solution.py:15
  197.7 5.3 %collective-permute-start = (f32[8,128,128]{2,1,0:T(8,128)S(1)}, f32[8,128,128]{2,1,0:T(8,128)S(1)}, u32[]{:S(2)}, u32[]{:S(2)}) collective-permute-start(f32[8,128,128]{2,1,0:T(8,128)S(1)} %convolution_add_fusion.12), channel_id=1, source_target_pairs={{0,4},{4,8},{8,12},{12,16},{16,20},{20,24},{24,28},{1,5},{5,9},{9,... | collective-permute-start | bytes 1572872 | tf_op jit(solution)/shard_map/while/body/eval_jaxpr/ppermute | solution.py:15
  203.0 6.6 %collective-permute-done = f32[8,128,128]{2,1,0:T(8,128)S(1)} collective-permute-done((f32[8,128,128]{2,1,0:T(8,128)S(1)}, f32[8,128,128]{2,1,0:T(8,128)S(1)}, u32[]{:S(2)}, u32[]{:S(2)}) %collective-permute-start) | collective-permute-done | bytes 524320 | tf_op jit(solution)/shard_map/while/body/eval_jaxpr/ppermute | solution.py:15
  209.6 1.3 fusion.45
  211.0 1.9 fusion.39
  215.1 1.0 fusion.59
  216.2 60.0 %reduce-scatter.2.cloned.1.call-done = bf16[2,4,16,128]{3,2,1,0:T(8,128)(2,1)} async-done(((bf16[2,4,128,128]{3,2,1,0:T(8,128)(2,1)}), bf16[2,4,16,128]{3,2,1,0:T(8,128)(2,1)}) %reduce-scatter.2.cloned.1.call-update) | async-done | bytes 32784 | tf_op jit(solution)/shard_map/reduce_scatter | solution.py:200
  276.1 0.9 fusion.76
  277.1 0.9 fusion.75
  278.0 19.8 %all-reduce = (f32[2,4,128]{2,1,0:T(4,128)S(1)}, f32[2,4,128]{2,1,0:T(4,128)S(1)}) all-reduce(f32[2,4,128]{2,1,0:T(4,128)S(1)} %bitcast.225, f32[2,4,128]{2,1,0:T(4,128)S(1)} %bitcast.226), channel_id=1, replica_groups=mesh['sp'=8,'tp'=4] {'sp'}, use_global_device_ids=true, to_apply=%region_13.14 | all-reduce | flops 2048 | bytes 16384 | tf_op jit(solution)/shard_map/psum | solution.py:206
  (105 shorter events, 19.7 us)
Async XLA Ops:
  7.2 33.7 %copy-start = (bf16[4096,4]{0,1:T(4,128)(2,1)S(1)}, bf16[4096,4]{0,1:T(4,128)(2,1)}, u32[]{:S(2)}) copy-start(bf16[4096,4]{0,1:T(4,128)(2,1)} %param.25) | copy-start | bytes 98308
  7.2 33.7 %all-gather.2.cloned.1.call-start = ((), (), s32[]{:S(2)}) async-start(), calls=%async_computation.1 | async-start | bytes 3932160 | tf_op jit(solution)/shard_map/all_gather | solution.py:136
  7.9 268.2 %reduce-scatter.2.cloned.1.call-start = ((), (), s32[]{:S(2)}) async-start(), calls=%async_computation.2 | async-start | bytes 294912 | tf_op jit(solution)/shard_map/reduce_scatter | solution.py:200
  44.6 5.9 %copy-start.1 = (bf16[2,192,4096]{2,1,0:T(8,128)(2,1)S(1)}, bf16[2,192,4096]{2,1,0:T(8,128)(2,1)}, u32[]{:S(2)}) copy-start(bf16[2,192,4096]{2,1,0:T(8,128)(2,1)} %all-gather.2.cloned.1.call-done) | copy-start | bytes 9437188
  44.7 5.9 %copy-start.13 = (bf16[4096,512]{1,0:T(8,128)(2,1)S(1)}, bf16[4096,512]{1,0:T(8,128)(2,1)}, u32[]{:S(2)}) copy-start(bf16[4096,512]{1,0:T(8,128)(2,1)} %param.20) | copy-start | bytes 12582916
  52.4 1.0 copy-start.5
  52.4 1.0 copy-start.11
  67.5 1.5 copy-start.6
  85.0 3.3 %copy-start.2 = (f32[3,8,64,64]{3,2,0,1:T(8,128)S(1)}, f32[3,8,64,64]{3,2,0,1:T(8,128)}, u32[]{:S(2)}) copy-start(f32[3,8,64,64]{3,2,0,1:T(8,128)} %get-tuple-element.397) | copy-start | bytes 1179652 | tf_op jit(solution)/shard_map/while
  92.8 3.3 %copy-start.2 = (f32[3,8,64,64]{3,2,0,1:T(8,128)S(1)}, f32[3,8,64,64]{3,2,0,1:T(8,128)}, u32[]{:S(2)}) copy-start(f32[3,8,64,64]{3,2,0,1:T(8,128)} %get-tuple-element.397) | copy-start | bytes 1179652 | tf_op jit(solution)/shard_map/while
  100.7 3.3 %copy-start.2 = (f32[3,8,64,64]{3,2,0,1:T(8,128)S(1)}, f32[3,8,64,64]{3,2,0,1:T(8,128)}, u32[]{:S(2)}) copy-start(f32[3,8,64,64]{3,2,0,1:T(8,128)} %get-tuple-element.397) | copy-start | bytes 1179652 | tf_op jit(solution)/shard_map/while
  108.5 102.5 %copy-start.3 = (f32[3,8,64,128]{3,2,0,1:T(8,128)S(1)}, f32[3,8,64,128]{3,2,0,1:T(8,128)}, u32[]{:S(2)}) copy-start(f32[3,8,64,128]{3,2,0,1:T(8,128)} %get-tuple-element.90) | copy-start | bytes 2359300
  109.2 14.9 %collective-permute-start = (f32[8,128,128]{2,1,0:T(8,128)S(1)}, f32[8,128,128]{2,1,0:T(8,128)S(1)}, u32[]{:S(2)}, u32[]{:S(2)}) collective-permute-start(f32[8,128,128]{2,1,0:T(8,128)S(1)} %convolution_add_fusion.12), channel_id=1, source_target_pairs={{0,4},{4,8},{8,12},{12,16},{16,20},{20,24},{24,28},{1,5},{5,9},{9,... | collective-permute-start | bytes 1572872 | tf_op jit(solution)/shard_map/while/body/eval_jaxpr/ppermute | solution.py:15
  124.8 15.1 %collective-permute-start = (f32[8,128,128]{2,1,0:T(8,128)S(1)}, f32[8,128,128]{2,1,0:T(8,128)S(1)}, u32[]{:S(2)}, u32[]{:S(2)}) collective-permute-start(f32[8,128,128]{2,1,0:T(8,128)S(1)} %convolution_add_fusion.12), channel_id=1, source_target_pairs={{0,4},{4,8},{8,12},{12,16},{16,20},{20,24},{24,28},{1,5},{5,9},{9,... | collective-permute-start | bytes 1572872 | tf_op jit(solution)/shard_map/while/body/eval_jaxpr/ppermute | solution.py:15
  140.6 14.2 %collective-permute-start = (f32[8,128,128]{2,1,0:T(8,128)S(1)}, f32[8,128,128]{2,1,0:T(8,128)S(1)}, u32[]{:S(2)}, u32[]{:S(2)}) collective-permute-start(f32[8,128,128]{2,1,0:T(8,128)S(1)} %convolution_add_fusion.12), channel_id=1, source_target_pairs={{0,4},{4,8},{8,12},{12,16},{16,20},{20,24},{24,28},{1,5},{5,9},{9,... | collective-permute-start | bytes 1572872 | tf_op jit(solution)/shard_map/while/body/eval_jaxpr/ppermute | solution.py:15
  155.5 14.2 %collective-permute-start = (f32[8,128,128]{2,1,0:T(8,128)S(1)}, f32[8,128,128]{2,1,0:T(8,128)S(1)}, u32[]{:S(2)}, u32[]{:S(2)}) collective-permute-start(f32[8,128,128]{2,1,0:T(8,128)S(1)} %convolution_add_fusion.12), channel_id=1, source_target_pairs={{0,4},{4,8},{8,12},{12,16},{16,20},{20,24},{24,28},{1,5},{5,9},{9,... | collective-permute-start | bytes 1572872 | tf_op jit(solution)/shard_map/while/body/eval_jaxpr/ppermute | solution.py:15
  170.3 13.4 %collective-permute-start = (f32[8,128,128]{2,1,0:T(8,128)S(1)}, f32[8,128,128]{2,1,0:T(8,128)S(1)}, u32[]{:S(2)}, u32[]{:S(2)}) collective-permute-start(f32[8,128,128]{2,1,0:T(8,128)S(1)} %convolution_add_fusion.12), channel_id=1, source_target_pairs={{0,4},{4,8},{8,12},{12,16},{16,20},{20,24},{24,28},{1,5},{5,9},{9,... | collective-permute-start | bytes 1572872 | tf_op jit(solution)/shard_map/while/body/eval_jaxpr/ppermute | solution.py:15
  184.4 12.6 %collective-permute-start = (f32[8,128,128]{2,1,0:T(8,128)S(1)}, f32[8,128,128]{2,1,0:T(8,128)S(1)}, u32[]{:S(2)}, u32[]{:S(2)}) collective-permute-start(f32[8,128,128]{2,1,0:T(8,128)S(1)} %convolution_add_fusion.12), channel_id=1, source_target_pairs={{0,4},{4,8},{8,12},{12,16},{16,20},{20,24},{24,28},{1,5},{5,9},{9,... | collective-permute-start | bytes 1572872 | tf_op jit(solution)/shard_map/while/body/eval_jaxpr/ppermute | solution.py:15
  197.7 12.0 %collective-permute-start = (f32[8,128,128]{2,1,0:T(8,128)S(1)}, f32[8,128,128]{2,1,0:T(8,128)S(1)}, u32[]{:S(2)}, u32[]{:S(2)}) collective-permute-start(f32[8,128,128]{2,1,0:T(8,128)S(1)} %convolution_add_fusion.12), channel_id=1, source_target_pairs={{0,4},{4,8},{8,12},{12,16},{16,20},{20,24},{24,28},{1,5},{5,9},{9,... | collective-permute-start | bytes 1572872 | tf_op jit(solution)/shard_map/while/body/eval_jaxpr/ppermute | solution.py:15
  213.3 1.9 copy-start.4
  213.8 62.4 %copy-start.9 = (f32[2,4,16]{2,1,0:T(4,128)S(1)}, f32[2,4,16]{2,1,0:T(4,128)}, u32[]{:S(2)}) copy-start(f32[2,4,16]{2,1,0:T(4,128)} %get-tuple-element.259) | copy-start | bytes 1540
  213.8 63.3 %copy-start.8 = (f32[2,4,16]{2,1,0:T(4,128)S(1)}, f32[2,4,16]{2,1,0:T(4,128)}, u32[]{:S(2)}) copy-start(f32[2,4,16]{2,1,0:T(4,128)} %get-tuple-element.260) | copy-start | bytes 1540
  213.8 83.9 %copy-start.7 = (bf16[2,4,128]{2,1,0:T(4,128)(2,1)S(1)}, bf16[2,4,128]{2,1,0:T(4,128)(2,1)}, u32[]{:S(2)}) copy-start(bf16[2,4,128]{2,1,0:T(4,128)(2,1)} %param.31) | copy-start | bytes 6148
  213.8 83.9 %copy-start.10 = (f32[2,4]{1,0:T(2,128)S(1)}, f32[2,4]{1,0:T(2,128)}, u32[]{:S(2)}) copy-start(f32[2,4]{1,0:T(2,128)} %param.33) | copy-start | bytes 100
  213.8 84.1 %copy-start.12 = (f32[128]{0:T(128)S(1)}, f32[128]{0:T(128)}, u32[]{:S(2)}) copy-start(f32[128]{0:T(128)} %param.28) | copy-start | bytes 1540
Sparse Core Ops, SparseCore 0:
  9.5 31.2 all-gather.1
  211.1 64.9 reduce-scatter.1
where the time goes:
time: 306 us; the launch traced here: 305 us
  waiting for transfers between devices  151 us (49%)
  matrix products  71.6 us (23%)
  starting transfers between devices  33.5 us (11%)
  blocking collectives  19.8 us (6%)
  between operations  14.5 us (5%)
  other arithmetic  9.26 us (3%)
  local copies, waits for them, and re-layouts  5.57 us (2%)
    ppermute x7, waiting for transfers between devices, shifted(): lax.ppermute(value, axis, [(source, source + steps) for source in range(f...  63 us
    reduce_scatter x1, waiting for transfers between devices, shards(): lax.psum_scatter(own_term.astype(jnp.bfloat16), 'sp', scatter_dimension=2...  60 us
    dot_general x49, matrix products, matmul(): return jnp.einsum(form, left, right, precision=highest)  48.5 us
    ppermute x7, starting transfers between devices, shifted(): lax.ppermute(value, axis, [(source, source + steps) for source in range(f...  33.4 us
    all_gather x1, waiting for transfers between devices, shards(): lax.all_gather(tokens, 'tp', axis=2, tiled=True)  27.1 us
    dot_general x6, matrix products, project_rows(): jnp.dot(flat_rows, weight, preferred_element_type=jnp.float32)  23.1 us
    psum x1, blocking collectives, shards(): lax.psum((matmul('shde,shd->she', memory, query_part), matmul('shde,shd->...  19.8 us
  transfers between devices with their start and end apart: 9, of which 9 were waited for; matrix products, arithmetic and copies ran while one was open for 4% of the time, Pallas kernels for 0%

commit v1 on v0

--- a/solution.py
+++ b/solution.py
@@ -7,6 +7,17 @@
 unit_floor = 1.0
 norm_floor = 0.001
 highest = lax.Precision.HIGHEST
+
+
+def gather_around(array, axis, dim):
+    ways = lax.axis_size(axis)
+    pieces = [array]
+    for far in range(1, ways):
+        pieces.append(
+            lax.ppermute(pieces[far - 1], axis, [(d, (d - 1) % ways) for d in range(ways)])
+        )
+    line = jnp.concatenate(pieces, axis=dim)
+    return jnp.roll(line, lax.axis_index(axis) * array.shape[dim], axis=dim)
 
 
 def shifted(value, axis, steps):
@@ -133,7 +144,7 @@
     seq_count, span_len, _ = tokens.shape
     head_count = rate_log.shape[0]
     weights = (query_weight, key_weight, value_weight, gate_weight, beta_weight, decay_weight)
-    totals = project_rows(lax.all_gather(tokens, "tp", axis=2, tiled=True), weights)
+    totals = project_rows(gather_around(tokens, "tp", 2), weights)
     query_rows = stored(totals[0])
     key_rows = stored(totals[1])
     value_rows = stored(totals[2])

time: 306 us -> 320 us (1.046)
  starting transfers between devices: 33.5 us -> 39.7 us
  matrix products: 71.6 us -> 75.5 us
  local copies, waits for them, and re-layouts: 5.57 us -> 9.2 us
    all_gather x1 -> x0, waiting for transfers between devices: 27.1 us -> none  [shards(): lax.all_gather(tokens, 'tp', axis=2, tiled=True)]
    ppermute x0 -> x3, waiting for transfers between devices: none -> 21.7 us  [gather_around(): lax.ppermute(pieces[far - 1], axis, [(d, (d - 1) % ways) for d in range(w...]
    ppermute x0 -> x3, starting transfers between devices: none -> 6.19 us  [gather_around(): lax.ppermute(pieces[far - 1], axis, [(d, (d - 1) % ways) for d in range(w...]
    dot_general x49, matrix products: 48.5 us -> 54.2 us  [matmul(): return jnp.einsum(form, left, right, precision=highest)]
    reduce_scatter x1, waiting for transfers between devices: 60 us -> 63.4 us  [shards(): lax.psum_scatter(own_term.astype(jnp.bfloat16), 'sp', scatter_dimension=2...]
    unnamed x27 -> x38, local copies, waits for them, and re-layouts: 0.69 us -> 3.92 us
  transfers between devices with their start and end apart: 9 -> 11, of which waited for: 9 -> 11; matrix products, arithmetic and copies ran while one was open for 4% -> 4% of each run, Pallas kernels for 0% -> 0%
where the time goes in v1:
time: 320 us; the launch traced here: 319 us
  waiting for transfers between devices  151 us (47%)
  matrix products  75.5 us (24%)
  starting transfers between devices  39.7 us (12%)
  blocking collectives  19.7 us (6%)
  between operations  14.6 us (5%)
  other arithmetic  9.24 us (3%)
  local copies, waits for them, and re-layouts  9.2 us (3%)
    ppermute x7, waiting for transfers between devices, shifted(): lax.ppermute(value, axis, [(source, source + steps) for source in range(f...  66 us
    reduce_scatter x1, waiting for transfers between devices, shards(): lax.psum_scatter(own_term.astype(jnp.bfloat16), 'sp', scatter_dimension=2...  63.4 us
    dot_general x49, matrix products, matmul(): return jnp.einsum(form, left, right, precision=highest)  54.2 us
    ppermute x7, starting transfers between devices, shifted(): lax.ppermute(value, axis, [(source, source + steps) for source in range(f...  33.5 us
    ppermute x3, waiting for transfers between devices, gather_around(): lax.ppermute(pieces[far - 1], axis, [(d, (d - 1) % ways) for d in range(w...  21.7 us
    dot_general x6, matrix products, project_rows(): jnp.dot(flat_rows, weight, preferred_element_type=jnp.float32)  21.2 us
    psum x1, blocking collectives, shards(): lax.psum((matmul('shde,shd->she', memory, query_part), matmul('shde,shd->...  19.7 us
  transfers between devices with their start and end apart: 11, of which 11 were waited for; matrix products, arithmetic and copies ran while one was open for 4% of the time, Pallas kernels for 0%

profile of v1, /device:TPU:0, one launch (start us, length us, event | category | flops | bytes accessed | tf_op | source)
XLA Modules:
  0.0 319.4 jit_solution(11661704949225231169)
XLA Ops:
  7.2 2.5 collective-permute-start.1
  11.3 8.3 %collective-permute-done.1 = bf16[2,192,1024]{2,1,0:T(8,128)(2,1)S(1)} collective-permute-done((bf16[2,192,1024]{2,1,0:T(8,128)(2,1)}, bf16[2,192,1024]{2,1,0:T(8,128)(2,1)S(1)}, u32[]{:S(2)}, u32[]{:S(2)}) %collective-permute-start.1) | collective-permute-done | bytes 786464 | tf_op jit(solution)/shard_map/ppermute | solution.py:17
  19.5 1.8 collective-permute-start.2
  23.6 1.2 constant_dynamic-update-slice_fusion.7
  25.4 5.4 %collective-permute-done.2 = bf16[2,192,1024]{2,1,0:T(8,128)(2,1)S(1)} collective-permute-done((bf16[2,192,1024]{2,1,0:T(8,128)(2,1)S(1)}, bf16[2,192,1024]{2,1,0:T(8,128)(2,1)S(1)}, u32[]{:S(2)}, u32[]{:S(2)}) %collective-permute-start.2) | collective-permute-done | bytes 786464 | tf_op jit(solution)/shard_map/ppermute | solution.py:17
  30.9 1.9 collective-permute-start.3
  34.2 8.0 %collective-permute-done.3 = bf16[2,192,1024]{2,1,0:T(8,128)(2,1)S(1)} collective-permute-done((bf16[2,192,1024]{2,1,0:T(8,128)(2,1)S(1)}, bf16[2,192,1024]{2,1,0:T(8,128)(2,1)S(1)}, u32[]{:S(2)}, u32[]{:S(2)}) %collective-permute-start.3) | collective-permute-done | bytes 786464 | tf_op jit(solution)/shard_map/ppermute | solution.py:17
  43.0 1.7 copy-done.1
  44.7 0.9 fusion.66
  46.6 5.8 %convolution_convert_fusion = bf16[384,512]{1,0:T(8,128)(2,1)} fusion(bf16[384,4096]{1,0:T(8,128)(2,1)} %bitcast.200, bf16[4096,512]{1,0:T(8,128)(2,1)} %param.23), kind=kOutput, calls=%fused_computation.59 | convolution fusion | flops 1610809344 | bytes 7733248 | tf_op jit(solution)/shard_map/dot_general | solution.py:123
  52.5 1.8 convolution_convert_fusion.1
  55.3 2.8 fusion.49
  58.2 4.9 %convolution_convert_fusion.3 = bf16[384,512]{1,0:T(8,128)(2,1)S(1)} fusion(bf16[384,4096]{1,0:T(8,128)(2,1)} %bitcast.202, bf16[4096,512]{1,0:T(8,128)(2,1)} %param.21), kind=kOutput, calls=%fused_computation.62 | convolution fusion | flops 1610809344 | bytes 7733248 | tf_op jit(solution)/shard_map/dot_general | solution.py:123
  64.1 4.9 %convolution_convert_fusion.2 = bf16[384,512]{1,0:T(8,128)(2,1)S(1)} fusion(bf16[384,4096]{1,0:T(8,128)(2,1)} %bitcast.203, bf16[4096,512]{1,0:T(8,128)(2,1)} %param.22), kind=kOutput, calls=%fused_computation.61 | convolution fusion | flops 1610809344 | bytes 7733248 | tf_op jit(solution)/shard_map/dot_general | solution.py:123
  69.5 1.2 multiply_bitcast_fusion
  70.9 1.4 fusion.41
  72.4 0.9 fusion.70
  74.2 0.9 convolution_add_fusion.7
  76.1 0.9 convolution_add_fusion.6
  77.9 0.9 convolution_add_fusion.5
  79.7 0.9 convolution_add_fusion.4
  80.6 0.9 convolution_add_fusion.3
  81.6 2.0 convolution_bitcast_fusion.4
  83.6 0.9 convolution_bitcast_fusion.3
  84.5 2.3 fusion.38
  86.9 29.2 %while.28 = (s32[]{:T(128)}, f32[8,128,128]{2,1,0:T(8,128)S(1)}, f32[8,128,128]{2,1,0:T(8,128)S(1)}, f32[3,8,64,128]{3,2,0,1:T(8,128)}, f32[3,8,64,128]{3,2,0,1:...) while((s32[]{:T(128)}, f32[8,128,128]{2,1,0:T(8,128)S(1)}, ...), condition=%wide.region_4.5_spmd.clone, body=%wide.region_3.4_spmd.clone.sunk | while | flops 806420480 | bytes 10819816 | solution.py:185
  87.5 1.5 convolution_subtract_fusion.6
  89.1 1.1 convolution_add_fusion.13
  90.2 1.3 convolution_subtract_fusion.8
  91.6 1.3 fusion.170
  92.9 1.0 convolution_subtract_fusion.7
  94.6 2.1 fusion.169
  97.2 1.5 convolution_subtract_fusion.6
  98.8 1.1 convolution_add_fusion.13
  99.9 1.3 convolution_subtract_fusion.8
  101.3 1.3 fusion.170
  102.6 1.0 convolution_subtract_fusion.7
  104.3 2.1 fusion.169
  106.9 1.5 convolution_subtract_fusion.6
  108.5 1.1 convolution_add_fusion.13
  109.6 1.3 convolution_subtract_fusion.8
  111.0 1.3 fusion.170
  112.4 1.0 convolution_subtract_fusion.7
  114.0 2.0 fusion.169
  116.1 104.1 %while.27 = (s32[]{:T(128)}, f32[8,128,128]{2,1,0:T(8,128)S(1)}, f32[8,128,128]{2,1,0:T(8,128)S(1)}, f32[8,128,128]{2,1,0:T(8,128)S(1)}, s32[]{:T(128)}) while((s32[]{:T(128)}, f32[8,128,128]{2,1,0:T(8,128)S(1)}, f32[8,128,128]{2,1,0:T(8,128)S(1)}, f32[8,128,128]{2,1,0:T(8,128)S(1)}, s32[]{:T(128)}) %tuple.60), condition=%wide.region_6.7_spmd, body=%wide.region_5.6_spmd.sunk | while | flops 201457664 | bytes 4194405 | solution.py:193
  116.8 3.4 %collective-permute-start = (f32[8,128,128]{2,1,0:T(8,128)S(1)}, f32[8,128,128]{2,1,0:T(8,128)S(1)}, u32[]{:S(2)}, u32[]{:S(2)}) collective-permute-start(f32[8,128,128]{2,1,0:T(8,128)S(1)} %convolution_add_fusion.12), channel_id=1, source_target_pairs={{0,4},{4,8},{8,12},{12,16},{16,20},{20,24},{24,28},{1,5},{5,9},{9,... | collective-permute-start | bytes 1572872 | tf_op jit(solution)/shard_map/while/body/eval_jaxpr/ppermute | solution.py:26
  120.2 12.0 %collective-permute-done = f32[8,128,128]{2,1,0:T(8,128)S(1)} collective-permute-done((f32[8,128,128]{2,1,0:T(8,128)S(1)}, f32[8,128,128]{2,1,0:T(8,128)S(1)}, u32[]{:S(2)}, u32[]{:S(2)}) %collective-permute-start) | collective-permute-done | bytes 524320 | tf_op jit(solution)/shard_map/while/body/eval_jaxpr/ppermute | solution.py:26
  132.9 4.4 %collective-permute-start = (f32[8,128,128]{2,1,0:T(8,128)S(1)}, f32[8,128,128]{2,1,0:T(8,128)S(1)}, u32[]{:S(2)}, u32[]{:S(2)}) collective-permute-start(f32[8,128,128]{2,1,0:T(8,128)S(1)} %convolution_add_fusion.12), channel_id=1, source_target_pairs={{0,4},{4,8},{8,12},{12,16},{16,20},{20,24},{24,28},{1,5},{5,9},{9,... | collective-permute-start | bytes 1572872 | tf_op jit(solution)/shard_map/while/body/eval_jaxpr/ppermute | solution.py:26
  137.3 11.1 %collective-permute-done = f32[8,128,128]{2,1,0:T(8,128)S(1)} collective-permute-done((f32[8,128,128]{2,1,0:T(8,128)S(1)}, f32[8,128,128]{2,1,0:T(8,128)S(1)}, u32[]{:S(2)}, u32[]{:S(2)}) %collective-permute-start) | collective-permute-done | bytes 524320 | tf_op jit(solution)/shard_map/while/body/eval_jaxpr/ppermute | solution.py:26
  149.1 4.4 %collective-permute-start = (f32[8,128,128]{2,1,0:T(8,128)S(1)}, f32[8,128,128]{2,1,0:T(8,128)S(1)}, u32[]{:S(2)}, u32[]{:S(2)}) collective-permute-start(f32[8,128,128]{2,1,0:T(8,128)S(1)} %convolution_add_fusion.12), channel_id=1, source_target_pairs={{0,4},{4,8},{8,12},{12,16},{16,20},{20,24},{24,28},{1,5},{5,9},{9,... | collective-permute-start | bytes 1572872 | tf_op jit(solution)/shard_map/while/body/eval_jaxpr/ppermute | solution.py:26
  153.5 10.3 %collective-permute-done = f32[8,128,128]{2,1,0:T(8,128)S(1)} collective-permute-done((f32[8,128,128]{2,1,0:T(8,128)S(1)}, f32[8,128,128]{2,1,0:T(8,128)S(1)}, u32[]{:S(2)}, u32[]{:S(2)}) %collective-permute-start) | collective-permute-done | bytes 524320 | tf_op jit(solution)/shard_map/while/body/eval_jaxpr/ppermute | solution.py:26
  164.5 5.3 %collective-permute-start = (f32[8,128,128]{2,1,0:T(8,128)S(1)}, f32[8,128,128]{2,1,0:T(8,128)S(1)}, u32[]{:S(2)}, u32[]{:S(2)}) collective-permute-start(f32[8,128,128]{2,1,0:T(8,128)S(1)} %convolution_add_fusion.12), channel_id=1, source_target_pairs={{0,4},{4,8},{8,12},{12,16},{16,20},{20,24},{24,28},{1,5},{5,9},{9,... | collective-permute-start | bytes 1572872 | tf_op jit(solution)/shard_map/while/body/eval_jaxpr/ppermute | solution.py:26
  169.8 9.4 %collective-permute-done = f32[8,128,128]{2,1,0:T(8,128)S(1)} collective-permute-done((f32[8,128,128]{2,1,0:T(8,128)S(1)}, f32[8,128,128]{2,1,0:T(8,128)S(1)}, u32[]{:S(2)}, u32[]{:S(2)}) %collective-permute-start) | collective-permute-done | bytes 524320 | tf_op jit(solution)/shard_map/while/body/eval_jaxpr/ppermute | solution.py:26
  179.8 5.3 %collective-permute-start = (f32[8,128,128]{2,1,0:T(8,128)S(1)}, f32[8,128,128]{2,1,0:T(8,128)S(1)}, u32[]{:S(2)}, u32[]{:S(2)}) collective-permute-start(f32[8,128,128]{2,1,0:T(8,128)S(1)} %convolution_add_fusion.12), channel_id=1, source_target_pairs={{0,4},{4,8},{8,12},{12,16},{16,20},{20,24},{24,28},{1,5},{5,9},{9,... | collective-permute-start | bytes 1572872 | tf_op jit(solution)/shard_map/while/body/eval_jaxpr/ppermute | solution.py:26
  185.2 8.6 %collective-permute-done = f32[8,128,128]{2,1,0:T(8,128)S(1)} collective-permute-done((f32[8,128,128]{2,1,0:T(8,128)S(1)}, f32[8,128,128]{2,1,0:T(8,128)S(1)}, u32[]{:S(2)}, u32[]{:S(2)}) %collective-permute-start) | collective-permute-done | bytes 524320 | tf_op jit(solution)/shard_map/while/body/eval_jaxpr/ppermute | solution.py:26
  194.4 5.3 %collective-permute-start = (f32[8,128,128]{2,1,0:T(8,128)S(1)}, f32[8,128,128]{2,1,0:T(8,128)S(1)}, u32[]{:S(2)}, u32[]{:S(2)}) collective-permute-start(f32[8,128,128]{2,1,0:T(8,128)S(1)} %convolution_add_fusion.12), channel_id=1, source_target_pairs={{0,4},{4,8},{8,12},{12,16},{16,20},{20,24},{24,28},{1,5},{5,9},{9,... | collective-permute-start | bytes 1572872 | tf_op jit(solution)/shard_map/while/body/eval_jaxpr/ppermute | solution.py:26
  199.7 7.7 %collective-permute-done = f32[8,128,128]{2,1,0:T(8,128)S(1)} collective-permute-done((f32[8,128,128]{2,1,0:T(8,128)S(1)}, f32[8,128,128]{2,1,0:T(8,128)S(1)}, u32[]{:S(2)}, u32[]{:S(2)}) %collective-permute-start) | collective-permute-done | bytes 524320 | tf_op jit(solution)/shard_map/while/body/eval_jaxpr/ppermute | solution.py:26
  208.1 5.3 %collective-permute-start = (f32[8,128,128]{2,1,0:T(8,128)S(1)}, f32[8,128,128]{2,1,0:T(8,128)S(1)}, u32[]{:S(2)}, u32[]{:S(2)}) collective-permute-start(f32[8,128,128]{2,1,0:T(8,128)S(1)} %convolution_add_fusion.12), channel_id=1, source_target_pairs={{0,4},{4,8},{8,12},{12,16},{16,20},{20,24},{24,28},{1,5},{5,9},{9,... | collective-permute-start | bytes 1572872 | tf_op jit(solution)/shard_map/while/body/eval_jaxpr/ppermute | solution.py:26
  213.4 6.9 %collective-permute-done = f32[8,128,128]{2,1,0:T(8,128)S(1)} collective-permute-done((f32[8,128,128]{2,1,0:T(8,128)S(1)}, f32[8,128,128]{2,1,0:T(8,128)S(1)}, u32[]{:S(2)}, u32[]{:S(2)}) %collective-permute-start) | collective-permute-done | bytes 524320 | tf_op jit(solution)/shard_map/while/body/eval_jaxpr/ppermute | solution.py:26
  220.2 1.3 fusion.45
  221.6 1.9 fusion.39
  225.7 1.0 fusion.59
  226.7 63.4 %reduce-scatter.2.cloned.1.call-done = bf16[2,4,16,128]{3,2,1,0:T(8,128)(2,1)} async-done(((bf16[2,4,128,128]{3,2,1,0:T(8,128)(2,1)}), bf16[2,4,16,128]{3,2,1,0:T(8,128)(2,1)}) %reduce-scatter.2.cloned.1.call-update) | async-done | bytes 32784 | tf_op jit(solution)/shard_map/reduce_scatter | solution.py:211
  292.0 19.7 %all-reduce = (f32[2,4,128]{2,1,0:T(4,128)S(1)}, f32[2,4,128]{2,1,0:T(4,128)S(1)}) all-reduce(f32[2,4,128]{2,1,0:T(4,128)S(1)} %bitcast.225, f32[2,4,128]{2,1,0:T(4,128)S(1)} %bitcast.226), channel_id=1, replica_groups=mesh['sp'=8,'tp'=4] {'sp'}, use_global_device_ids=true, to_apply=%region_13.14 | all-reduce | flops 2048 | bytes 16384 | tf_op jit(solution)/shard_map/psum | solution.py:217
  (115 shorter events, 27.1 us)
Async XLA Ops:
  7.2 37.5 %copy-start = (bf16[4096,4]{0,1:T(4,128)(2,1)S(1)}, bf16[4096,4]{0,1:T(4,128)(2,1)}, u32[]{:S(2)}) copy-start(bf16[4096,4]{0,1:T(4,128)(2,1)} %param.25) | copy-start | bytes 98308
  7.2 35.2 %copy-start.3 = (bf16[2,192,1024]{2,1,0:T(8,128)(2,1)S(1)}, bf16[2,192,1024]{2,1,0:T(8,128)(2,1)}, u32[]{:S(2)}) copy-start(bf16[2,192,1024]{2,1,0:T(8,128)(2,1)} %param.19) | copy-start | bytes 2359300
  7.2 283.0 %reduce-scatter.2.cloned.1.call-start = ((), (), s32[]{:S(2)}) async-start(), calls=%async_computation.1 | async-start | bytes 294912 | tf_op jit(solution)/shard_map/reduce_scatter | solution.py:211
  7.2 12.3 %collective-permute-start.1 = (bf16[2,192,1024]{2,1,0:T(8,128)(2,1)}, bf16[2,192,1024]{2,1,0:T(8,128)(2,1)S(1)}, u32[]{:S(2)}, u32[]{:S(2)}) collective-permute-start(bf16[2,192,1024]{2,1,0:T(8,128)(2,1)} %param.19), channel_id=1, source_target_pairs={{0,3},{1,0},{2,1},{3,2},{4,7},{5,4},{6,5},{7,6},{8,11},{9,8},{10,9... | collective-permute-start | bytes 2359304 | tf_op jit(solution)/shard_map/ppermute | solution.py:17
  19.5 11.3 %collective-permute-start.2 = (bf16[2,192,1024]{2,1,0:T(8,128)(2,1)S(1)}, bf16[2,192,1024]{2,1,0:T(8,128)(2,1)S(1)}, u32[]{:S(2)}, u32[]{:S(2)}) collective-permute-start(bf16[2,192,1024]{2,1,0:T(8,128)(2,1)S(1)} %collective-permute-done.1), channel_id=1, source_target_pairs={{0,3},{1,0},{2,1},{3,2},{4,7},{5,4},{6,5},{7,6},{8,11},{9,8},{10,9... | collective-permute-start | bytes 2359304 | tf_op jit(solution)/shard_map/ppermute | solution.py:17
  30.9 11.4 %collective-permute-start.3 = (bf16[2,192,1024]{2,1,0:T(8,128)(2,1)S(1)}, bf16[2,192,1024]{2,1,0:T(8,128)(2,1)S(1)}, u32[]{:S(2)}, u32[]{:S(2)}) collective-permute-start(bf16[2,192,1024]{2,1,0:T(8,128)(2,1)S(1)} %collective-permute-done.2), channel_id=1, source_target_pairs={{0,3},{1,0},{2,1},{3,2},{4,7},{5,4},{6,5},{7,6},{8,11},{9,8},{10,9... | collective-permute-start | bytes 2359304 | tf_op jit(solution)/shard_map/ppermute | solution.py:17
  43.0 1.7 copy-start.1
  46.5 5.9 %copy-start.2 = (bf16[2,192,4096]{2,1,0:T(8,128)(2,1)S(1)}, bf16[2,192,4096]{2,1,0:T(8,128)(2,1)}, u32[]{:S(2)}) copy-start(bf16[2,192,4096]{2,1,0:T(8,128)(2,1)} %copy-done.1) | copy-start | bytes 9437188
  46.6 5.9 %copy-start.14 = (bf16[4096,512]{1,0:T(8,128)(2,1)S(1)}, bf16[4096,512]{1,0:T(8,128)(2,1)}, u32[]{:S(2)}) copy-start(bf16[4096,512]{1,0:T(8,128)(2,1)} %param.20) | copy-start | bytes 12582916
  54.3 1.0 copy-start.6
  54.3 1.0 copy-start.12
  69.4 1.5 copy-start.7
  116.1 105.5 %copy-start.4 = (f32[3,8,64,128]{3,2,0,1:T(8,128)S(1)}, f32[3,8,64,128]{3,2,0,1:T(8,128)}, u32[]{:S(2)}) copy-start(f32[3,8,64,128]{3,2,0,1:T(8,128)} %get-tuple-element.90) | copy-start | bytes 2359300
  116.8 15.4 %collective-permute-start = (f32[8,128,128]{2,1,0:T(8,128)S(1)}, f32[8,128,128]{2,1,0:T(8,128)S(1)}, u32[]{:S(2)}, u32[]{:S(2)}) collective-permute-start(f32[8,128,128]{2,1,0:T(8,128)S(1)} %convolution_add_fusion.12), channel_id=1, source_target_pairs={{0,4},{4,8},{8,12},{12,16},{16,20},{20,24},{24,28},{1,5},{5,9},{9,... | collective-permute-start | bytes 1572872 | tf_op jit(solution)/shard_map/while/body/eval_jaxpr/ppermute | solution.py:26
  132.9 15.6 %collective-permute-start = (f32[8,128,128]{2,1,0:T(8,128)S(1)}, f32[8,128,128]{2,1,0:T(8,128)S(1)}, u32[]{:S(2)}, u32[]{:S(2)}) collective-permute-start(f32[8,128,128]{2,1,0:T(8,128)S(1)} %convolution_add_fusion.12), channel_id=1, source_target_pairs={{0,4},{4,8},{8,12},{12,16},{16,20},{20,24},{24,28},{1,5},{5,9},{9,... | collective-permute-start | bytes 1572872 | tf_op jit(solution)/shard_map/while/body/eval_jaxpr/ppermute | solution.py:26
  149.1 14.7 %collective-permute-start = (f32[8,128,128]{2,1,0:T(8,128)S(1)}, f32[8,128,128]{2,1,0:T(8,128)S(1)}, u32[]{:S(2)}, u32[]{:S(2)}) collective-permute-start(f32[8,128,128]{2,1,0:T(8,128)S(1)} %convolution_add_fusion.12), channel_id=1, source_target_pairs={{0,4},{4,8},{8,12},{12,16},{16,20},{20,24},{24,28},{1,5},{5,9},{9,... | collective-permute-start | bytes 1572872 | tf_op jit(solution)/shard_map/while/body/eval_jaxpr/ppermute | solution.py:26
  164.5 14.7 %collective-permute-start = (f32[8,128,128]{2,1,0:T(8,128)S(1)}, f32[8,128,128]{2,1,0:T(8,128)S(1)}, u32[]{:S(2)}, u32[]{:S(2)}) collective-permute-start(f32[8,128,128]{2,1,0:T(8,128)S(1)} %convolution_add_fusion.12), channel_id=1, source_target_pairs={{0,4},{4,8},{8,12},{12,16},{16,20},{20,24},{24,28},{1,5},{5,9},{9,... | collective-permute-start | bytes 1572872 | tf_op jit(solution)/shard_map/while/body/eval_jaxpr/ppermute | solution.py:26
  179.8 13.9 %collective-permute-start = (f32[8,128,128]{2,1,0:T(8,128)S(1)}, f32[8,128,128]{2,1,0:T(8,128)S(1)}, u32[]{:S(2)}, u32[]{:S(2)}) collective-permute-start(f32[8,128,128]{2,1,0:T(8,128)S(1)} %convolution_add_fusion.12), channel_id=1, source_target_pairs={{0,4},{4,8},{8,12},{12,16},{16,20},{20,24},{24,28},{1,5},{5,9},{9,... | collective-permute-start | bytes 1572872 | tf_op jit(solution)/shard_map/while/body/eval_jaxpr/ppermute | solution.py:26
  194.4 13.0 %collective-permute-start = (f32[8,128,128]{2,1,0:T(8,128)S(1)}, f32[8,128,128]{2,1,0:T(8,128)S(1)}, u32[]{:S(2)}, u32[]{:S(2)}) collective-permute-start(f32[8,128,128]{2,1,0:T(8,128)S(1)} %convolution_add_fusion.12), channel_id=1, source_target_pairs={{0,4},{4,8},{8,12},{12,16},{16,20},{20,24},{24,28},{1,5},{5,9},{9,... | collective-permute-start | bytes 1572872 | tf_op jit(solution)/shard_map/while/body/eval_jaxpr/ppermute | solution.py:26
  208.1 12.2 %collective-permute-start = (f32[8,128,128]{2,1,0:T(8,128)S(1)}, f32[8,128,128]{2,1,0:T(8,128)S(1)}, u32[]{:S(2)}, u32[]{:S(2)}) collective-permute-start(f32[8,128,128]{2,1,0:T(8,128)S(1)} %convolution_add_fusion.12), channel_id=1, source_target_pairs={{0,4},{4,8},{8,12},{12,16},{16,20},{20,24},{24,28},{1,5},{5,9},{9,... | collective-permute-start | bytes 1572872 | tf_op jit(solution)/shard_map/while/body/eval_jaxpr/ppermute | solution.py:26
  223.6 2.2 copy-start.5
  223.9 66.3 %copy-start.10 = (f32[2,4,16]{2,1,0:T(4,128)S(1)}, f32[2,4,16]{2,1,0:T(4,128)}, u32[]{:S(2)}) copy-start(f32[2,4,16]{2,1,0:T(4,128)} %get-tuple-element.259) | copy-start | bytes 1540
  223.9 67.2 %copy-start.9 = (f32[2,4,16]{2,1,0:T(4,128)S(1)}, f32[2,4,16]{2,1,0:T(4,128)}, u32[]{:S(2)}) copy-start(f32[2,4,16]{2,1,0:T(4,128)} %get-tuple-element.260) | copy-start | bytes 1540
  223.9 87.8 %copy-start.8 = (bf16[2,4,128]{2,1,0:T(4,128)(2,1)S(1)}, bf16[2,4,128]{2,1,0:T(4,128)(2,1)}, u32[]{:S(2)}) copy-start(bf16[2,4,128]{2,1,0:T(4,128)(2,1)} %param.31) | copy-start | bytes 6148
  223.9 87.8 %copy-start.11 = (f32[2,4]{1,0:T(2,128)S(1)}, f32[2,4]{1,0:T(2,128)}, u32[]{:S(2)}) copy-start(f32[2,4]{1,0:T(2,128)} %param.33) | copy-start | bytes 100
  223.9 88.0 %copy-start.13 = (f32[128]{0:T(128)S(1)}, f32[128]{0:T(128)}, u32[]{:S(2)}) copy-start(f32[128]{0:T(128)} %param.28) | copy-start | bytes 1540
Sparse Core Ops, SparseCore 0:
  221.7 68.3 reduce-scatter.1
